TPU v7x, 512 devices: a whole 4x8x8 slice. The times are simulated.
512 devices in a mesh: sp: 32 (over z, x), tp: 16 (over y, core).
Axes of the slice: x: 4, y: 8, z: 8, core: 2. Of those that a mesh axis runs over, the one named last changes fastest.
Arguments:
- pool_input: bfloat16 [1024, 12288], P('tp', 'sp'), may hold values from -6 to 6
- pool_gate: bfloat16 [1024, 12288], P('tp', 'sp'), may hold values from -6 to 6
- pool_mix: bfloat16 [4, 256, 256], replicated, may hold values from -0.375 to 0.375
- pool_scale: float32 [1024], replicated, may hold values from 0.1 to 1.9
- out_proj: bfloat16 [1024, 2048], P(None, 'tp'), may hold values from -0.375 to 0.375
- residual: bfloat16 [12288, 2048], P('sp', 'tp'), may hold values from -12 to 12
- norm_gain: float32 [2048], P('tp'), may hold values from 0.1 to 1.9
- routes: int32 [12288, 2], P('sp'), may hold values from 0 to 31, all different within a row; in each aligned block of 384 rows (0 to 383, 384 to 767, ...) at most 36 rows name the same one
- group_logits: float32 [12288, 4], P('sp'), may hold values from -4 to 4
- expert_scores: float32 [12288, 2], P('sp'), may hold values from -4 to 4
- w_gate: bfloat16 [32, 2048, 4096], P('sp', None, 'tp'), may hold values from -0.125 to 0.125
- w_up: bfloat16 [32, 2048, 4096], P('sp', None, 'tp'), may hold values from -0.125 to 0.125
- w_down: bfloat16 [32, 4096, 2048], P('sp', None, 'tp'), may hold values from -0.375 to 0.375
Outputs:
- layer_out: bfloat16 [12288, 2048], P('sp', 'tp')
Inputs may be any that keep to these rules, and one draw needn't show every extreme that they name: `routes`: among the rows of one device (aligned blocks of 384 rows) no expert is named by more than 36 rows, a bound that some block reaches; the 2 experts of a row differ.
All inputs are finite; a program needn't handle non-finite values.
Results may differ from a plain program's by a relative error of at most 0.01.
Values may be sent and summed in bfloat16 or wider, within the bound.
No kernel may reach another device: no remote copies, remote signals or barrier semaphores. Data moves between devices by JAX's collectives and lax.ppermute only.
A program may use at most 64 MiB of HBM per device.

v0:
```python
import jax
import jax.numpy as jnp
from jax import lax
from jax.sharding import PartitionSpec as P

D = 2048
POOL_GROUP = 256
TOP = 2
reach_back = 15
epsilon = 1e-06


def from_behind(value, axis, steps):
    count = lax.axis_size(axis)
    initial, last = (max(0, -steps), min(count, count - steps))
    return lax.ppermute(value, axis, [(source, source + steps) for source in range(initial, last)])


def in_one_piece(arrays, axis, dim, along):
    ends, at = ([], 0)
    for a in arrays[:-1]:
        at += a.shape[along]
        ends.append(at)
    both = jnp.concatenate(arrays, axis=along)
    return tuple(jnp.split(lax.all_gather(both, axis, axis=dim, tiled=True), ends, axis=along))


def from_everyone(value, axis):
    count = lax.axis_size(axis)
    return lax.all_to_all(
        jnp.broadcast_to(value[None], (count, *value.shape)), axis, 0, 0, tiled=True
    )


def over_copies(value, axis):
    return from_everyone(value, axis).sum(axis=0)


def window_terms(extended, first_channel, first_position, group_width):
    length = extended.shape[1] - reach_back
    layered = extended
    stride = 1
    partial_sums = []
    for _ in range(4):
        layered = layered[:, stride:] + layered[:, :-stride]
        stride = stride * 2
        partial_sums.append(layered[:, layered.shape[1] - length :])
    channel = first_channel + jnp.arange(extended.shape[0], dtype=jnp.int32)
    scale_index = channel // group_width
    chosen = partial_sums[3]
    for octave in range(3):
        chosen = jnp.where((scale_index == octave)[:, None], partial_sums[octave], chosen)
    window = (2 ** (scale_index + 1)).astype(jnp.float32)
    positions = (first_position + jnp.arange(length, dtype=jnp.int32) + 1).astype(jnp.float32)
    counted = jnp.minimum(positions[None, :], window[:, None])
    return chosen / counted - extended[:, reach_back:]


def slot_table(row_block, experts, capacity):
    flattened = row_block.reshape(-1)
    onehot = (flattened[:, None] == jnp.arange(experts, dtype=jnp.int32)[None, :]).astype(jnp.int32)
    before = jnp.cumsum(onehot, axis=0) - onehot
    ranked = jnp.sum(before * onehot, axis=1)
    return flattened * capacity + ranked


def route_weights(routes, group_logits, expert_scores, per_group):
    raised = jnp.exp(group_logits)
    group_prob = raised / jnp.sum(raised, axis=1, keepdims=True)
    owning_group = routes // per_group
    groups_iota = jnp.arange(group_logits.shape[1], dtype=jnp.int32)
    picked = jnp.sum(
        jnp.where(
            owning_group[:, :, None] == groups_iota[None, None, :], group_prob[:, None, :], 0.0
        ),
        axis=2,
    )
    lifted = jnp.exp(expert_scores)
    return picked * lifted / jnp.sum(lifted, axis=1, keepdims=True)


def per_device(
    pool_input,
    pool_gate,
    pool_mix,
    pool_scale,
    out_proj,
    residual,
    norm_gain,
    routes,
    group_logits,
    expert_scores,
    w_gate,
    w_up,
    w_down,
):
    channels, length = pool_input.shape
    edge_rows = from_behind(pool_input[:, length - reach_back :], "sp", 1)
    extended = jnp.concatenate([edge_rows, pool_input], axis=1).astype(jnp.float32)
    first_channel = lax.axis_index("tp") * channels
    first_position = lax.axis_index("sp") * length
    pooled = window_terms(extended, first_channel, first_position, POOL_GROUP).astype(jnp.bfloat16)
    gathered, gate_rows = in_one_piece((pooled, pool_gate), "tp", 0, 1)
    scales = pool_mix.shape[0]
    mixed_rows = jnp.einsum(
        "gct,gcd->tgd",
        gathered.reshape(scales, POOL_GROUP, length),
        pool_mix,
        preferred_element_type=jnp.float32,
    ).reshape(length, scales * POOL_GROUP)
    branch = (
        jax.nn.sigmoid(gate_rows.T.astype(jnp.float32)) * mixed_rows * pool_scale[None, :]
    ).astype(jnp.bfloat16)
    hidden_state = (
        residual.astype(jnp.float32) + jnp.dot(branch, out_proj, preferred_element_type=jnp.float32)
    ).astype(jnp.bfloat16)
    state_float = hidden_state.astype(jnp.float32)
    squares = over_copies(jnp.sum(state_float * state_float, axis=1), "tp")
    normed = (state_float * lax.rsqrt(squares / D + epsilon)[:, None] * norm_gain[None, :]).astype(
        jnp.bfloat16
    )
    experts = lax.axis_size("sp") * w_gate.shape[0]
    weights = route_weights(routes, group_logits, expert_scores, experts // group_logits.shape[1])
    capacity = 3 * TOP * length // (2 * experts)
    destination = slot_table(routes, experts, capacity)
    token_index = jnp.arange(length * TOP, dtype=jnp.int32) // TOP
    sources = jnp.full((experts * capacity,), length, jnp.int32).at[destination].set(token_index)
    padded = jnp.concatenate([normed, jnp.zeros((1, normed.shape[1]), jnp.bfloat16)], axis=0)
    arrived = lax.all_to_all(padded[sources], "sp", split_axis=0, concat_axis=0, tiled=True)
    portion = lax.all_gather(arrived, "tp", axis=1, tiled=True)
    rows_gate = w_gate[0]
    rows_up = w_up[0]
    gate_term = jnp.dot(portion, rows_gate, preferred_element_type=jnp.float32)
    up_term = jnp.dot(portion, rows_up, preferred_element_type=jnp.float32)
    activated = (jax.nn.silu(gate_term) * up_term).astype(jnp.bfloat16)
    rows_down = w_down[0]
    result = jnp.dot(
        lax.all_gather(activated, "tp", axis=1, tiled=True),
        rows_down,
        preferred_element_type=jnp.float32,
    ).astype(jnp.bfloat16)
    returned = lax.all_to_all(result, "sp", split_axis=0, concat_axis=0, tiled=True)
    picked = returned[destination].astype(jnp.float32).reshape(length, TOP, returned.shape[1])
    combined = jnp.sum(weights[:, :, None] * picked, axis=1)
    return (state_float + combined).astype(jnp.bfloat16)


def solution(mesh):
    placed = (
        P("tp", "sp"),
        P("tp", "sp"),
        P(),
        P(),
        P(None, "tp"),
        P("sp", "tp"),
        P("tp"),
        P("sp", None),
        P("sp", None),
        P("sp", None),
        P("sp", None, "tp"),
        P("sp", None, "tp"),
        P("sp", None, "tp"),
    )
    return jax.shard_map(
        per_device, mesh=mesh, in_specs=placed, out_specs=P("sp", "tp"), check_vma=False
    )
```

profile of v0, /device:TPU:16, one launch (start us, length us, event | category | flops | bytes accessed | tf_op | source)
XLA Modules:
  0.0 268.7 jit_solution(10977367310961019468)
XLA Ops:
  6.5 0.9 slice.43
  7.4 3.4 %collective-permute-start = (bf16[64,15]{1,0:T(8,128)(2,1)S(1)}, bf16[64,15]{1,0:T(8,128)(2,1)S(1)}, u32[]{:S(2)}, u32[]{:S(2)}) collective-permute-start(bf16[64,15]{1,0:T(8,128)(2,1)S(1)} %slice.43), channel_id=1, source_target_pairs={{0,16},{16,32},{32,48},{48,64},{64,80},{80,96},{96,112},{112,128},... | collective-permute-start | bytes 5768 | tf_op jit(solution)/shard_map/ppermute | solution.py:16
  10.9 1.3 collective-permute-done
  12.2 0.9 maximum_convert_fusion
  13.1 0.1 slice_add_fusion.2
  13.2 0.1 slice_add_fusion.1
  13.3 0.1 slice_add_fusion
  13.5 0.2 fusion.13
  13.7 0.7 pad_maximum_fusion
  14.4 0.1 copy.36
  14.5 0.1 eq.69
  14.7 0.1 eq.65
  14.8 1.7 reduce-window.6
  16.6 0.3 slice_reduce_fusion
  16.9 0.1 copy.35
  17.0 0.2 mul.134
  17.2 0.1 fusion.12
  17.3 3.4 %scatter_custom_fusion = s32[1152]{0:T(1024)S(1)} fusion(s32[768]{0:T(1024)S(1)} %fusion.24, s32[768]{0:T(1024)S(1)} %add_select_fusion, s32[]{:T(128)} %constant.90.clone.1), kind=kCustom, calls=%fused_computation.60 | custom fusion | bytes 4612 | tf_op jit(solution)/shard_map/scatter | solution.py:127
  20.7 39.9 %all-gather.4.cloned.1.call-done = bf16[1024,768]{1,0:T(8,128)(2,1)} async-done(((bf16[64,768]{1,0:T(8,128)(2,1)}), bf16[1024,768]{1,0:T(8,128)(2,1)}) %all-gather.4.cloned.1.call-update) | async-done | bytes 1572880 | tf_op jit(solution)/shard_map/all_gather | solution.py:25
  60.7 1.6 slice-done
  62.3 0.5 fusion.26
  62.8 0.4 fusion.2
  63.3 0.5 copy-done.3
  63.7 0.0 copy-done.4
  63.8 0.5 multiply_reduce_fusion
  64.3 0.6 broadcast_in_dim.69
  64.9 6.4 %all-to-all-start = ((f32[16,1,384]{2,1,0:T(1,128)}), f32[16,1,384]{2,1,0:T(1,128)S(1)}, u32[]{:S(2)}, u32[]{:S(2)}) async-start(f32[16,1,384]{2,1,0:T(1,128)} %broadcast_in_dim.69), calls=%async_computation | async-start | bytes 49152 | tf_op jit(solution)/shard_map/all_to_all | solution.py:30
  71.3 0.0 all-gather.6.cloned.1.call-start
  71.3 5.4 %all-to-all-done = f32[16,1,384]{2,1,0:T(1,128)S(1)} async-done(((f32[16,1,384]{2,1,0:T(1,128)}), f32[16,1,384]{2,1,0:T(1,128)S(1)}, u32[]{:S(2)}, u32[]{:S(2)}) %all-to-all-start) | async-done | bytes 24608 | tf_op jit(solution)/shard_map/all_to_all | solution.py:30
  76.8 0.1 multiply_convert_fusion
  76.9 2.9 %gather_fusion = bf16[1152,128]{1,0:T(8,128)(2,1)S(1)} fusion(bf16[385,128]{1,0:T(8,128)(2,1)S(1)} %concatenate.11, s32[2048]{0:T(1024)S(1)} %pad_clamp_fusion), kind=kCustom, calls=%fused_computation | custom fusion | bytes 594432 | tf_op jit(solution)/shard_map/gather | solution.py:129
  79.8 0.1 all_to_all.21
  79.9 24.5 %all_to_all.30 = bf16[32,36,128]{2,1,0:T(8,128)(2,1)S(1)} all-to-all(bf16[32,36,128]{2,1,0:T(8,128)(2,1)S(1)} %all_to_all.21), channel_id=1, replica_groups=mesh['sp'=32,'tp'=16] {'sp'}, dimensions={0} | all-to-all | bytes 589824 | tf_op jit(solution)/shard_map/all_to_all | solution.py:129
  104.4 0.8 all_to_all.23
  105.2 0.0 all-gather.8.cloned.1.call-start
  105.2 45.1 %all-gather.6.cloned.1.call-done = bf16[1152,2048]{1,0:T(8,128)(2,1)} async-done(((bf16[1152,128]{1,0:T(8,128)(2,1)}), bf16[1152,2048]{1,0:T(8,128)(2,1)}) %all-gather.6.cloned.1.call-update) | async-done | bytes 4718608 | tf_op jit(solution)/shard_map/all_gather | solution.py:130
  150.3 3.9 %fusion.7 = f32[1152,256]{1,0:T(8,128)S(1)} fusion(bf16[1152,2048]{1,0:T(8,128)(2,1)} %all-gather.6.cloned.1.call-done, bf16[1,2048,256]{2,1,0:T(8,128)(2,1)S(1)} %copy-done), kind=kOutput, calls=%fused_computation.14 | convolution fusion | flops 1207959552 | bytes 6946816 | tf_op jit(solution)/shard_map/dot_general | solution.py:133
  154.2 2.3 fusion
  156.7 71.4 %all-gather.8.cloned.1.call-done = bf16[1152,4096]{1,0:T(8,128)(2,1)} async-done(((bf16[1152,256]{1,0:T(8,128)(2,1)}), bf16[1152,4096]{1,0:T(8,128)(2,1)}) %all-gather.8.cloned.1.call-update) | async-done | bytes 9437200 | tf_op jit(solution)/shard_map/all_gather | solution.py:138
  228.1 6.5 %convolution_convert_fusion = bf16[1152,128]{1,0:T(8,128)(2,1)S(1)} fusion(bf16[1152,4096]{1,0:T(8,128)(2,1)} %all-gather.8.cloned.1.call-done, bf16[1,4096,128]{2,1,0:T(8,128)(2,1)} %param.25), kind=kOutput, calls=%fused_computation.5 | convolution fusion | flops 1208107008 | bytes 10780672 | tf_op jit(solution)/shard_map/dot_general | solution.py:137
  234.6 0.8 all_to_all.24
  235.3 9.0 %all-to-all-start.2 = ((bf16[32,36,128]{2,1,0:T(8,128)(2,1)}), bf16[32,36,128]{2,1,0:T(8,128)(2,1)S(1)}, u32[]{:S(2)}, u32[]{:S(2)}) async-start(bf16[32,36,128]{2,1,0:T(8,128)(2,1)} %all_to_all.24), calls=%async_computation.2 | async-start | bytes 655360 | tf_op jit(solution)/shard_map/all_to_all | solution.py:142
  244.4 0.1 copy.33
  244.6 14.4 %all-to-all-done.2 = bf16[32,36,128]{2,1,0:T(8,128)(2,1)S(1)} async-done(((bf16[32,36,128]{2,1,0:T(8,128)(2,1)}), bf16[32,36,128]{2,1,0:T(8,128)(2,1)S(1)}, u32[]{:S(2)}, u32[]{:S(2)}) %all-to-all-start.2) | async-done | bytes 294944 | tf_op jit(solution)/shard_map/all_to_all | solution.py:142
  259.0 0.1 all_to_all.26
  259.0 1.9 gather_fusion.1
  260.9 0.6 fusion.9
  261.5 0.7 add_convert_fusion
  (49 shorter events, 0.4 us)
Async XLA Ops:
  6.5 143.8 %copy-start = (bf16[1,2048,256]{2,1,0:T(8,128)(2,1)S(1)}, bf16[1,2048,256]{2,1,0:T(8,128)(2,1)}, u32[]{:S(2)}) copy-start(bf16[1,2048,256]{2,1,0:T(8,128)(2,1)} %param.23) | copy-start | bytes 3145732
  6.5 7.1 %copy-start.5 = (bf16[64,384]{1,0:T(8,128)(2,1)S(1)}, bf16[64,384]{1,0:T(8,128)(2,1)}, u32[]{:S(2)}) copy-start(bf16[64,384]{1,0:T(8,128)(2,1)} %param.14) | copy-start | bytes 147460
  6.5 7.8 %copy-start.8 = (s32[384,2]{0,1:T(2,128)S(1)}, s32[384,2]{0,1:T(2,128)}, u32[]{:S(2)}) copy-start(s32[384,2]{0,1:T(2,128)} %param.20) | copy-start | bytes 9220
  6.5 54.1 %all-gather.4.cloned.1.call-start = ((), (), s32[]{:S(2)}) async-start(), calls=%async_computation.3 | async-start | bytes 1671168 | tf_op jit(solution)/shard_map/all_gather | solution.py:25
  7.4 4.8 %collective-permute-start = (bf16[64,15]{1,0:T(8,128)(2,1)S(1)}, bf16[64,15]{1,0:T(8,128)(2,1)S(1)}, u32[]{:S(2)}, u32[]{:S(2)}) collective-permute-start(bf16[64,15]{1,0:T(8,128)(2,1)S(1)} %slice.43), channel_id=1, source_target_pairs={{0,16},{16,32},{32,48},{48,64},{64,80},{80,96},{96,112},{112,128},... | collective-permute-start | bytes 5768 | tf_op jit(solution)/shard_map/ppermute | solution.py:16
  14.4 46.3 %copy-start.2 = (bf16[4,256,256]{2,1,0:T(8,128)(2,1)S(1)}, bf16[4,256,256]{2,1,0:T(8,128)(2,1)}, u32[]{:S(2)}) copy-start(bf16[4,256,256]{2,1,0:T(8,128)(2,1)} %param.15) | copy-start | bytes 1572868
  60.6 1.6 slice-start
  60.7 2.1 copy-start.1
  60.7 2.1 copy-start.9
  62.8 1.0 copy-start.3
  62.8 1.0 copy-start.4
  62.8 13.9 %copy-start.10 = (f32[128]{0:T(128)S(1)}, f32[128]{0:T(128)}, u32[]{:S(2)}) copy-start(f32[128]{0:T(128)} %param.19) | copy-start | bytes 1540
  64.9 11.8 %all-to-all-start = ((f32[16,1,384]{2,1,0:T(1,128)}), f32[16,1,384]{2,1,0:T(1,128)S(1)}, u32[]{:S(2)}, u32[]{:S(2)}) async-start(f32[16,1,384]{2,1,0:T(1,128)} %broadcast_in_dim.69), calls=%async_computation | async-start | bytes 49152 | tf_op jit(solution)/shard_map/all_to_all | solution.py:30
  71.3 79.0 %all-gather.6.cloned.1.call-start = ((), (), s32[]{:S(2)}) async-start(), calls=%async_computation.4 | async-start | bytes 5013504 | tf_op jit(solution)/shard_map/all_gather | solution.py:130
  105.2 49.0 %copy-start.12 = (bf16[1,2048,256]{2,1,0:T(8,128)(2,1)S(1)}, bf16[1,2048,256]{2,1,0:T(8,128)(2,1)}, u32[]{:S(2)}) copy-start(bf16[1,2048,256]{2,1,0:T(8,128)(2,1)} %param.24) | copy-start | bytes 3145732
  105.2 122.9 %all-gather.8.cloned.1.call-start = ((), (), s32[]{:S(2)}) async-start(), calls=%async_computation.5 | async-start | bytes 10027008 | tf_op jit(solution)/shard_map/all_gather | solution.py:138
  150.3 3.9 %copy-start.11 = (bf16[1152,2048]{1,0:T(8,128)(2,1)S(1)}, bf16[1152,2048]{1,0:T(8,128)(2,1)}, u32[]{:S(2)}) copy-start(bf16[1152,2048]{1,0:T(8,128)(2,1)} %all-gather.6.cloned.1.call-done) | copy-start | bytes 14155780
  154.2 2.4 copy-start.6
  156.7 87.7 %copy-start.7 = (f32[384,2]{0,1:T(2,128)S(1)}, f32[384,2]{0,1:T(2,128)}, u32[]{:S(2)}) copy-start(f32[384,2]{0,1:T(2,128)} %param.22) | copy-start | bytes 9220
  235.3 23.6 %all-to-all-start.2 = ((bf16[32,36,128]{2,1,0:T(8,128)(2,1)}), bf16[32,36,128]{2,1,0:T(8,128)(2,1)S(1)}, u32[]{:S(2)}, u32[]{:S(2)}) async-start(bf16[32,36,128]{2,1,0:T(8,128)(2,1)} %all_to_all.24), calls=%async_computation.2 | async-start | bytes 655360 | tf_op jit(solution)/shard_map/all_to_all | solution.py:142
Sparse Core Ops, SparseCore 0:
  14.5 46.1 all-gather.3
  105.3 44.9 all-gather.5
  156.7 71.2 all-gather.7
where the time goes:
time: 269 us
  waiting for transfers between devices  178 us (66%)
  blocking collectives  24.5 us (9%)
  starting transfers between devices  18.8 us (7%)
  local copies, waits for them, and re-layouts  14.7 us (5%)
  matrix products  13.7 us (5%)
  between operations  13.5 us (5%)
  other arithmetic  5.95 us (2%)
    all_gather x1, waiting for transfers between devices, per_device(): lax.all_gather(activated, 'tp', axis=1, tiled=True)  71.4 us
    all_gather x1, waiting for transfers between devices, per_device(): portion = lax.all_gather(arrived, 'tp', axis=1, tiled=True)  45.1 us
    all_gather x1, waiting for transfers between devices, in_one_piece(): lax.all_gather(both, axis, axis=dim, tiled=True)  39.9 us
    all_to_all x1, blocking collectives, per_device(): lax.all_to_all(padded[sources], 'sp', split_axis=0, concat_axis=0, tiled=...  24.5 us
    all_to_all x1, waiting for transfers between devices, per_device(): lax.all_to_all(result, 'sp', split_axis=0, concat_axis=0, tiled=True)  14.4 us
    all_to_all x1, starting transfers between devices, per_device(): lax.all_to_all(result, 'sp', split_axis=0, concat_axis=0, tiled=True)  8.98 us
    dot_general x1, matrix products, per_device(): jnp.dot(lax.all_gather(activated, 'tp', axis=1, tiled=True), rows_down, p...  6.52 us
    all_to_all x1, starting transfers between devices, from_everyone(): lax.all_to_all(jnp.broadcast_to(value[None], (count, *value.shape)), axis...  6.36 us
  transfers between devices with their start and end apart: 6, of which 6 were waited for; matrix products, arithmetic and copies ran while one was open for 2% of the time, Pallas kernels for 0%

commit v1 on v0

--- a/solution.py
+++ b/solution.py
@@ -1,3 +1,4 @@
+import functools
 import jax
 import jax.numpy as jnp
 from jax import lax
@@ -8,6 +9,18 @@
 TOP = 2
 reach_back = 15
 epsilon = 1e-06
+
+
+def create_digits(vector, net_axis, array_dim):
+    axis_len = lax.axis_size(net_axis)
+    copies = [axis_len if dd == array_dim else 1 for dd in range(vector.ndim)]
+    side_arr = jnp.tile(vector, copies)
+    return lax.all_to_all(
+        side_arr, net_axis, tiled=True, split_axis=array_dim, concat_axis=array_dim
+    )
+
+
+ticks_unite = functools.partial(create_digits, net_axis="tp", array_dim=1)
 
 
 def from_behind(value, axis, steps):
@@ -134,11 +147,9 @@
     up_term = jnp.dot(portion, rows_up, preferred_element_type=jnp.float32)
     activated = (jax.nn.silu(gate_term) * up_term).astype(jnp.bfloat16)
     rows_down = w_down[0]
-    result = jnp.dot(
-        lax.all_gather(activated, "tp", axis=1, tiled=True),
-        rows_down,
-        preferred_element_type=jnp.float32,
-    ).astype(jnp.bfloat16)
+    result = jnp.dot(ticks_unite(activated), rows_down, preferred_element_type=jnp.float32).astype(
+        jnp.bfloat16
+    )
     returned = lax.all_to_all(result, "sp", split_axis=0, concat_axis=0, tiled=True)
     picked = returned[destination].astype(jnp.float32).reshape(length, TOP, returned.shape[1])
     combined = jnp.sum(weights[:, :, None] * picked, axis=1)

time: 269 us -> 428 us (1.59)
  the two profiles are of different devices: /device:TPU:16 before, /device:TPU:24 now
where the time goes in v1:
time: 428 us; the launch traced here: 427 us
  waiting for transfers between devices  313 us (73%)
  local copies, waits for them, and re-layouts  32 us (7%)
  starting transfers between devices  25 us (6%)
  blocking collectives  24.5 us (6%)
  between operations  13.8 us (3%)
  matrix products  12.8 us (3%)
  other arithmetic  5.95 us (1%)
    all_to_all x1, waiting for transfers between devices, create_digits(): lax.all_to_all(side_arr, net_axis, tiled=True, split_axis=array_dim, conc...  206 us
    all_gather x1, waiting for transfers between devices, per_device(): portion = lax.all_gather(arrived, 'tp', axis=1, tiled=True)  45.8 us
    all_gather x1, waiting for transfers between devices, in_one_piece(): lax.all_gather(both, axis, axis=dim, tiled=True)  41 us
    all_to_all x1, blocking collectives, per_device(): lax.all_to_all(padded[sources], 'sp', split_axis=0, concat_axis=0, tiled=...  24.5 us
    all_to_all x1, waiting for transfers between devices, per_device(): lax.all_to_all(result, 'sp', split_axis=0, concat_axis=0, tiled=True)  14.2 us
    all_to_all x1, local copies, waits for them, and re-layouts, create_digits(): lax.all_to_all(side_arr, net_axis, tiled=True, split_axis=array_dim, conc...  12.8 us
    all_to_all x1, starting transfers between devices, per_device(): lax.all_to_all(result, 'sp', split_axis=0, concat_axis=0, tiled=True)  9.07 us
  transfers between devices with their start and end apart: 6, of which 6 were waited for; matrix products, arithmetic and copies ran while one was open for 2% of the time, Pallas kernels for 0%

profile of v1, /device:TPU:24, one launch (start us, length us, event | category | flops | bytes accessed | tf_op | source)
XLA Modules:
  0.0 427.0 jit_solution(15807973357118824054)
XLA Ops:
  6.5 0.9 slice.43
  7.4 3.4 collective-permute-start
  10.9 1.3 collective-permute-done
  12.2 0.9 maximum_convert_fusion
  13.1 0.1 slice_add_fusion.2
  13.2 0.1 slice_add_fusion.1
  13.3 0.1 slice_add_fusion
  13.5 0.2 fusion.13
  13.7 0.7 pad_maximum_fusion
  14.4 0.1 copy.54
  14.5 0.1 eq.69
  14.7 0.1 eq.65
  14.8 1.7 reduce-window.6
  16.6 0.3 slice_reduce_fusion
  16.9 0.1 copy.53
  17.0 0.2 mul.134
  17.2 0.1 fusion.12
  17.3 3.4 scatter_custom_fusion
  20.7 41.0 %all-gather.3.cloned.1.call-done = bf16[1024,768]{1,0:T(8,128)(2,1)} async-done(((bf16[64,768]{1,0:T(8,128)(2,1)}), bf16[1024,768]{1,0:T(8,128)(2,1)}) %all-gather.3.cloned.1.call-update) | async-done | bytes 1572880 | tf_op jit(solution)/shard_map/all_gather | solution.py:38
  61.8 1.6 slice-done
  63.4 0.5 fusion.26
  64.0 0.4 fusion.2
  64.4 0.5 copy-done.3
  64.9 0.5 multiply_reduce_fusion
  65.4 0.6 broadcast_in_dim.69
  66.0 5.1 %all-to-all-start = ((f32[16,1,384]{2,1,0:T(1,128)}), f32[16,1,384]{2,1,0:T(1,128)S(1)}, u32[]{:S(2)}, u32[]{:S(2)}) async-start(f32[16,1,384]{2,1,0:T(1,128)} %broadcast_in_dim.69), calls=%async_computation | async-start | bytes 49152 | tf_op jit(solution)/shard_map/all_to_all | solution.py:43
  71.2 4.5 %all-to-all-done = f32[16,1,384]{2,1,0:T(1,128)S(1)} async-done(((f32[16,1,384]{2,1,0:T(1,128)}), f32[16,1,384]{2,1,0:T(1,128)S(1)}, u32[]{:S(2)}, u32[]{:S(2)}) %all-to-all-start) | async-done | bytes 24608 | tf_op jit(solution)/shard_map/all_to_all | solution.py:43
  75.8 0.1 multiply_convert_fusion
  75.9 2.9 gather_fusion
  78.8 0.1 all_to_all.27
  78.9 24.5 %all_to_all.39 = bf16[32,36,128]{2,1,0:T(8,128)(2,1)S(1)} all-to-all(bf16[32,36,128]{2,1,0:T(8,128)(2,1)S(1)} %all_to_all.27), channel_id=1, replica_groups=mesh['sp'=32,'tp'=16] {'sp'}, dimensions={0} | all-to-all | bytes 589824 | tf_op jit(solution)/shard_map/all_to_all | solution.py:142
  103.4 0.8 all_to_all.29
  104.2 45.8 %all-gather.5.cloned.1.call-done = bf16[1152,2048]{1,0:T(8,128)(2,1)} async-done(((bf16[1152,128]{1,0:T(8,128)(2,1)}), bf16[1152,2048]{1,0:T(8,128)(2,1)}) %all-gather.5.cloned.1.call-update) | async-done | bytes 4718608 | tf_op jit(solution)/shard_map/all_gather | solution.py:143
  150.0 3.9 fusion.7
  153.9 1.6 fusion
  155.5 4.6 %tile.2 = bf16[1152,16,256]{2,0,1:T(8,128)(2,1)} broadcast(bf16[1152,256]{1,0:T(8,128)(2,1)S(1)} %fusion), dimensions={0,2} | broadcast | bytes 10027008 | tf_op jit(solution)/shard_map/tile | solution.py:17
  160.1 7.4 %all-to-all-start.2 = ((bf16[1152,16,256]{2,0,1:T(8,128)(2,1)}), bf16[1152,16,256]{2,0,1:T(8,128)(2,1)}, u32[]{:S(2)}, u32[]{:S(2)}) async-start(bf16[1152,16,256]{2,0,1:T(8,128)(2,1)} %tile.2), calls=%async_computation.2 | async-start | bytes 18874368 | tf_op jit(solution)/shard_map/all_to_all | solution.py:18
  167.5 206.0 %all-to-all-done.2 = bf16[1152,16,256]{2,0,1:T(8,128)(2,1)} async-done(((bf16[1152,16,256]{2,0,1:T(8,128)(2,1)}), bf16[1152,16,256]{2,0,1:T(8,128)(2,1)}, u32[]{:S(2)}, u32[]{:S(2)}) %all-to-all-start.2) | async-done | bytes 9437216 | tf_op jit(solution)/shard_map/all_to_all | solution.py:18
  373.5 12.8 %copy.57 = bf16[1152,16,256]{0,2,1:T(8,128)(2,1)} copy(bf16[1152,16,256]{2,0,1:T(8,128)(2,1)} %all-to-all-done.2) | data formatting | bytes 18874368 | tf_op jit(solution)/shard_map/all_to_all | solution.py:18
  386.3 6.4 %convolution_convert_fusion = bf16[1152,128]{1,0:T(8,128)(2,1)S(1)} fusion(bf16[1152,4096]{0,1:T(8,128)(2,1)} %bitcast.50, bf16[1,4096,128]{2,1,0:T(8,128)(2,1)S(1)} %copy-done.13), kind=kOutput, calls=%fused_computation.5 | convolution fusion | flops 1208107008 | bytes 10780672 | tf_op jit(solution)/shard_map/dot_general | solution.py:150
  392.6 0.8 all_to_all.32
  393.4 9.1 %all-to-all-start.3 = ((bf16[32,36,128]{2,1,0:T(8,128)(2,1)}), bf16[32,36,128]{2,1,0:T(8,128)(2,1)S(1)}, u32[]{:S(2)}, u32[]{:S(2)}) async-start(bf16[32,36,128]{2,1,0:T(8,128)(2,1)} %all_to_all.32), calls=%async_computation.3 | async-start | bytes 655360 | tf_op jit(solution)/shard_map/all_to_all | solution.py:153
  402.6 0.1 copy.51
  402.7 14.2 %all-to-all-done.3 = bf16[32,36,128]{2,1,0:T(8,128)(2,1)S(1)} async-done(((bf16[32,36,128]{2,1,0:T(8,128)(2,1)}), bf16[32,36,128]{2,1,0:T(8,128)(2,1)S(1)}, u32[]{:S(2)}, u32[]{:S(2)}) %all-to-all-start.3) | async-done | bytes 294944 | tf_op jit(solution)/shard_map/all_to_all | solution.py:153
  417.0 0.1 all_to_all.34
  417.1 1.9 gather_fusion.1
  418.9 0.6 fusion.9
  419.5 0.7 add_convert_fusion
  (52 shorter events, 0.4 us)
Async XLA Ops:
  6.5 143.5 %copy-start = (bf16[1,2048,256]{2,1,0:T(8,128)(2,1)S(1)}, bf16[1,2048,256]{2,1,0:T(8,128)(2,1)}, u32[]{:S(2)}) copy-start(bf16[1,2048,256]{2,1,0:T(8,128)(2,1)} %param.23) | copy-start | bytes 3145732
  6.5 7.1 %copy-start.5 = (bf16[64,384]{1,0:T(8,128)(2,1)S(1)}, bf16[64,384]{1,0:T(8,128)(2,1)}, u32[]{:S(2)}) copy-start(bf16[64,384]{1,0:T(8,128)(2,1)} %param.14) | copy-start | bytes 147460
  6.5 7.8 %copy-start.8 = (s32[384,2]{0,1:T(2,128)S(1)}, s32[384,2]{0,1:T(2,128)}, u32[]{:S(2)}) copy-start(s32[384,2]{0,1:T(2,128)} %param.20) | copy-start | bytes 9220
  6.5 55.2 %all-gather.3.cloned.1.call-start = ((), (), s32[]{:S(2)}) async-start(), calls=%async_computation.4 | async-start | bytes 1671168 | tf_op jit(solution)/shard_map/all_gather | solution.py:38
  7.4 4.8 %collective-permute-start = (bf16[64,15]{1,0:T(8,128)(2,1)S(1)}, bf16[64,15]{1,0:T(8,128)(2,1)S(1)}, u32[]{:S(2)}, u32[]{:S(2)}) collective-permute-start(bf16[64,15]{1,0:T(8,128)(2,1)S(1)} %slice.43), channel_id=1, source_target_pairs={{0,16},{16,32},{32,48},{48,64},{64,80},{80,96},{96,112},{112,128},... | collective-permute-start | bytes 5768 | tf_op jit(solution)/shard_map/ppermute | solution.py:29
  14.4 47.4 %copy-start.2 = (bf16[4,256,256]{2,1,0:T(8,128)(2,1)S(1)}, bf16[4,256,256]{2,1,0:T(8,128)(2,1)}, u32[]{:S(2)}) copy-start(bf16[4,256,256]{2,1,0:T(8,128)(2,1)} %param.15) | copy-start | bytes 1572868
  61.8 1.6 slice-start
  61.8 2.1 copy-start.1
  61.8 2.1 copy-start.9
  63.9 1.0 copy-start.3
  63.9 1.0 copy-start.4
  64.0 11.8 %copy-start.10 = (f32[128]{0:T(128)S(1)}, f32[128]{0:T(128)}, u32[]{:S(2)}) copy-start(f32[128]{0:T(128)} %param.19) | copy-start | bytes 1540
  66.0 9.7 %all-to-all-start = ((f32[16,1,384]{2,1,0:T(1,128)}), f32[16,1,384]{2,1,0:T(1,128)S(1)}, u32[]{:S(2)}, u32[]{:S(2)}) async-start(f32[16,1,384]{2,1,0:T(1,128)} %broadcast_in_dim.69), calls=%async_computation | async-start | bytes 49152 | tf_op jit(solution)/shard_map/all_to_all | solution.py:43
  71.1 78.9 %all-gather.5.cloned.1.call-start = ((), (), s32[]{:S(2)}) async-start(), calls=%async_computation.5 | async-start | bytes 5013504 | tf_op jit(solution)/shard_map/all_gather | solution.py:143
  104.2 49.7 %copy-start.12 = (bf16[1,2048,256]{2,1,0:T(8,128)(2,1)S(1)}, bf16[1,2048,256]{2,1,0:T(8,128)(2,1)}, u32[]{:S(2)}) copy-start(bf16[1,2048,256]{2,1,0:T(8,128)(2,1)} %param.24) | copy-start | bytes 3145732
  150.0 3.9 copy-start.11
  160.1 7.4 %copy-start.6 = (f32[384,4]{0,1:T(4,128)S(1)}, f32[384,4]{0,1:T(4,128)}, u32[]{:S(2)}) copy-start(f32[384,4]{0,1:T(4,128)} %param.21) | copy-start | bytes 18436
  160.1 213.4 %all-to-all-start.2 = ((bf16[1152,16,256]{2,0,1:T(8,128)(2,1)}), bf16[1152,16,256]{2,0,1:T(8,128)(2,1)}, u32[]{:S(2)}, u32[]{:S(2)}) async-start(bf16[1152,16,256]{2,0,1:T(8,128)(2,1)} %tile.2), calls=%async_computation.2 | async-start | bytes 18874368 | tf_op jit(solution)/shard_map/all_to_all | solution.py:18
  167.5 218.8 %copy-start.13 = (bf16[1,4096,128]{2,1,0:T(8,128)(2,1)S(1)}, bf16[1,4096,128]{2,1,0:T(8,128)(2,1)}, u32[]{:S(2)}) copy-start(bf16[1,4096,128]{2,1,0:T(8,128)(2,1)} %param.25) | copy-start | bytes 3145732
  386.3 16.2 %copy-start.7 = (f32[384,2]{0,1:T(2,128)S(1)}, f32[384,2]{0,1:T(2,128)}, u32[]{:S(2)}) copy-start(f32[384,2]{0,1:T(2,128)} %param.22) | copy-start | bytes 9220
  393.4 23.6 %all-to-all-start.3 = ((bf16[32,36,128]{2,1,0:T(8,128)(2,1)}), bf16[32,36,128]{2,1,0:T(8,128)(2,1)S(1)}, u32[]{:S(2)}, u32[]{:S(2)}) async-start(bf16[32,36,128]{2,1,0:T(8,128)(2,1)} %all_to_all.32), calls=%async_computation.3 | async-start | bytes 655360 | tf_op jit(solution)/shard_map/all_to_all | solution.py:153
Sparse Core Ops, SparseCore 0:
  14.5 47.2 all-gather.2
  104.3 45.6 all-gather.4
